TPU v7x, 32 devices: a whole 2x2x4 slice. The times are simulated.
32 devices in a mesh: ep: 8 (over z, core), tp: 4 (over y, x).
Axes of the slice: x: 2, y: 2, z: 4, core: 2. Of those that a mesh axis runs over, the one named last changes fastest.
Arguments:
- mix_in: bfloat16 [2048, 2048], P('ep'), may hold values from -6 to 6
- mix_gain: float32 [2048], replicated, may hold values from 0.1 to 1.9
- w_in_x: bfloat16 [2048, 2048], P(None, 'tp'), may hold values from -0.125 to 0.125
- w_in_y: bfloat16 [2048, 2048], P(None, 'tp'), may hold values from -0.125 to 0.125
- conv_taps: float32 [4, 2048], P(None, 'tp'), may hold values from -3 to 3
- recur_gate_w: bfloat16 [16, 128, 128], P('tp'), may hold values from -0.5 to 0.5
- input_gate_w: bfloat16 [16, 128, 128], P('tp'), may hold values from -0.5 to 0.5
- decay_logit: float32 [2048], P('tp'), may hold values from 4 to 20
- decay_shift: float32 [2048, 2048], P('ep', 'tp'), may hold values from -2.2 to 0
- moe_in: bfloat16 [2048, 2048], P('ep'), may hold values from -6 to 6
- moe_gain: float32 [2048], replicated, may hold values from 0.1 to 1.9
- routes: int32 [2048, 2], P('ep'), may hold values from 0 to 7, all different within a row; in each aligned block of 256 rows (0 to 255, 256 to 511, ...) at most 128 rows name the same one
- route_weight: float32 [2048, 2], P('ep'), may hold values from 0.1 to 1
- expert_gate: bfloat16 [8, 2048, 2048], P('ep', None, 'tp'), may hold values from -0.125 to 0.125
- expert_up: bfloat16 [8, 2048, 2048], P('ep', None, 'tp'), may hold values from -0.125 to 0.125
- expert_down: bfloat16 [8, 2048, 2048], P('ep', None, 'tp'), may hold values from -0.125 to 0.125
Outputs:
- mixer_out: bfloat16 [2048, 2048], P('ep', 'tp')
- moe_out: bfloat16 [2048, 2048], P('ep', 'tp')
Inputs may be any that keep to these rules, and one draw needn't show every extreme that they name: `routes`: each row names 2 different experts. Among the rows of one index of ep no expert is named more than 128 times, a bound that some block reaches.
All inputs are finite; a program needn't handle non-finite values.
Results may differ from a plain program's by a relative error of at most 0.0095.
Values may be sent and summed in bfloat16 or wider, within the bound.
A program may use at most 64 MiB of HBM per device.

v0:
```python
import jax
import jax.numpy as jnp
from jax import lax
from jax.sharding import PartitionSpec as P

epsilon = 1e-06
lru_scale = 8.0


def from_behind(value, axis, by):
    count = lax.axis_size(axis)
    pairs = [(i, i + by) for i in range(count) if 0 <= i + by < count]
    return lax.ppermute(value, axis, pairs)


def entering(value, axis, combine, identity):
    count, index = (lax.axis_size(axis), lax.axis_index(axis))
    everything = jax.tree.map(lambda part: lax.all_gather(part, axis), value)
    start = jax.tree.map(
        lambda part, zero: jnp.broadcast_to(jnp.asarray(zero, part.dtype), part.shape),
        value,
        identity,
    )

    def hop(k, before):
        reached = k < index
        new = combine(before, jax.tree.map(lambda part: part[k], everything))
        return jax.tree.map(lambda a, b: jnp.where(reached, a, b), new, before)

    return lax.fori_loop(0, count, hop, start)


def norm_rows(rows, gain):
    widened = rows.astype(jnp.float32)
    scaled = widened * lax.rsqrt(jnp.mean(widened * widened, axis=-1, keepdims=True) + epsilon)
    return (scaled * gain[None, :]).astype(jnp.bfloat16)


def link(earlier, later):
    return (earlier[0] * later[0], later[0] * earlier[1] + later[1])


def local(
    mix_in,
    mix_gain,
    w_in_x,
    w_in_y,
    conv_taps,
    recur_gate_w,
    input_gate_w,
    decay_logit,
    decay_shift,
    moe_in,
    moe_gain,
    routes,
    route_weight,
    expert_gate,
    expert_up,
    expert_down,
):
    row_count = mix_in.shape[0]
    width_dev = w_in_x.shape[1]
    heads_dev = recur_gate_w.shape[0]
    block_size = recur_gate_w.shape[1]
    tap_count = conv_taps.shape[0]
    mixer_rows = norm_rows(mix_in, mix_gain)
    x_branch = jnp.dot(mixer_rows, w_in_x, preferred_element_type=jnp.float32).astype(jnp.bfloat16)
    y_branch = jnp.dot(mixer_rows, w_in_y, preferred_element_type=jnp.float32).astype(jnp.bfloat16)
    previous = from_behind(x_branch[row_count - (tap_count - 1) :], "ep", 1)
    padded = jnp.concatenate([previous, x_branch], axis=0)
    conv_sum = jnp.zeros((row_count, width_dev), jnp.float32)
    for tap_index in range(tap_count):
        conv_sum = conv_sum + conv_taps[tap_index][None, :] * padded[
            tap_index : tap_index + row_count
        ].astype(jnp.float32)
    x_conv = conv_sum.astype(jnp.bfloat16)
    heads_in = x_conv.reshape(row_count, heads_dev, block_size)
    gate_a = jnp.einsum(
        "thi,hij->thj", heads_in, recur_gate_w, preferred_element_type=jnp.float32
    ).reshape(row_count, width_dev)
    gate_x = jnp.einsum(
        "thi,hij->thj", heads_in, input_gate_w, preferred_element_type=jnp.float32
    ).reshape(row_count, width_dev)
    log_decay = (
        -lru_scale * jax.nn.sigmoid(gate_a) * jax.nn.softplus(-decay_logit)[None, :] + decay_shift
    )
    lru_drive = (
        jnp.sqrt(-jnp.expm1(2.0 * log_decay)) * jax.nn.sigmoid(gate_x) * x_conv.astype(jnp.float32)
    )
    through, local_state = lax.associative_scan(link, (jnp.exp(log_decay), lru_drive), axis=0)
    identity = (jnp.ones((width_dev,), jnp.float32), jnp.zeros((width_dev,), jnp.float32))
    carried = entering((through[row_count - 1], local_state[row_count - 1]), "ep", link, identity)
    lru_state = local_state + through * carried[1][None, :]
    mixer_out = (lru_state * jax.nn.gelu(y_branch.astype(jnp.float32))).astype(jnp.bfloat16)
    moe_rows = norm_rows(moe_in, moe_gain)
    token_count = moe_rows.shape[0]
    feature_count = moe_rows.shape[1]
    choose_count = routes.shape[1]
    expert_count = lax.axis_size("ep")
    capacity = 2 * token_count * choose_count // expert_count
    slot_total = expert_count * capacity
    expert_ids = routes.reshape(-1)
    onehot = (expert_ids[:, None] == jnp.arange(expert_count, dtype=jnp.int32)[None, :]).astype(
        jnp.int32
    )
    slot_rank = jnp.sum(jnp.cumsum(onehot, axis=0) * onehot, axis=1) - 1
    slot_index = expert_ids * capacity + slot_rank
    token_index = jnp.repeat(jnp.arange(token_count, dtype=jnp.int32), choose_count)
    slot_owner = jnp.full((slot_total,), token_count, jnp.int32).at[slot_index].set(token_index)
    padded_rows = jnp.concatenate([moe_rows, jnp.zeros((1, feature_count), jnp.bfloat16)], axis=0)
    outgoing = padded_rows[slot_owner].reshape(expert_count, capacity, feature_count)
    column_width = feature_count // lax.axis_size("tp")
    own_columns = lax.dynamic_slice_in_dim(
        outgoing, lax.axis_index("tp") * column_width, column_width, 2
    )
    incoming = lax.all_to_all(own_columns, "ep", split_axis=0, concat_axis=0, tiled=True)
    piece = lax.all_gather(incoming, "tp", axis=2, tiled=True)
    flat_rows = piece.reshape(slot_total, piece.shape[2])
    gate_rows = expert_gate[0]
    up_rows = expert_up[0]
    gate_proj = jnp.dot(flat_rows, gate_rows, preferred_element_type=jnp.float32)
    up_proj = jnp.dot(flat_rows, up_rows, preferred_element_type=jnp.float32)
    hidden = (jax.nn.silu(gate_proj) * up_proj).astype(jnp.bfloat16)
    down_rows = expert_down[0]
    columns = jnp.dot(
        lax.all_gather(hidden, "tp", axis=1, tiled=True),
        down_rows,
        preferred_element_type=jnp.float32,
    )
    results = columns.astype(jnp.bfloat16).reshape(expert_count, capacity, expert_down.shape[2])
    returned = lax.all_to_all(results, "ep", split_axis=0, concat_axis=0, tiled=True).reshape(
        slot_total, expert_down.shape[2]
    )
    picked = (
        returned[slot_index]
        .astype(jnp.float32)
        .reshape(token_count, choose_count, expert_down.shape[2])
    )
    route_share = route_weight / jnp.sum(route_weight, axis=1, keepdims=True)
    moe_out = jnp.sum(route_share[:, :, None] * picked, axis=1).astype(jnp.bfloat16)
    return (mixer_out, moe_out)


def solution(mesh):
    placed = (
        P("ep", None),
        P(),
        P(None, "tp"),
        P(None, "tp"),
        P(None, "tp"),
        P("tp", None, None),
        P("tp", None, None),
        P("tp"),
        P("ep", "tp"),
        P("ep", None),
        P(),
        P("ep", None),
        P("ep", None),
        P("ep", None, "tp"),
        P("ep", None, "tp"),
        P("ep", None, "tp"),
    )
    return jax.shard_map(
        local, mesh=mesh, in_specs=placed, out_specs=(P("ep", "tp"), P("ep", "tp")), check_vma=False
    )
```

profile of v0, /device:TPU:0, one launch (start us, length us, event | category | flops | bytes accessed | tf_op | source)
XLA Modules:
  0.0 283.7 jit_solution(14209495019624665678)
XLA Ops:
  11.2 2.4 scatter_custom_fusion
  13.6 1.5 fusion.3
  15.6 6.0 %gather_fusion = bf16[1024,2048]{1,0:T(8,128)(2,1)} fusion(bf16[257,2048]{1,0:T(8,128)(2,1)S(1)} %concatenate.63, s32[1024]{0:T(1024)S(1)} %fusion.50), kind=kCustom, calls=%fused_computation | custom fusion | bytes 8392704 | tf_op jit(solution)/shard_map/gather | solution.py:111
  22.9 33.0 %all_to_all.10 = bf16[8,128,512]{2,1,0:T(8,128)(2,1)} all-to-all(bf16[8,128,512]{2,1,0:T(8,128)(2,1)S(1)} %constant_dynamic-slice_fusion.2), channel_id=1, replica_groups=mesh['ep'=8,'tp'=4] {'ep'}, dimensions={0} | all-to-all | bytes 2097152 | tf_op jit(solution)/shard_map/all_to_all | solution.py:116
  56.8 2.4 convolution_convert_fusion.1
  59.9 1.5 collective-permute-start
  63.0 1.7 add_convert_fusion
  64.7 42.8 %all-gather.5.cloned.1.call-done = bf16[8,128,2048]{2,1,0:T(8,128)(2,1)} async-done(((bf16[8,128,512]{2,1,0:T(8,128)(2,1)}), bf16[8,128,2048]{2,1,0:T(8,128)(2,1)}) %all-gather.5.cloned.1.call-update) | async-done | bytes 4194320 | tf_op jit(solution)/shard_map/all_gather | solution.py:117
  107.4 4.7 %fusion.8 = f32[1024,512]{1,0:T(8,128)S(1)} fusion(bf16[1024,2048]{1,0:T(8,128)(2,1)} %bitcast.86, bf16[1,2048,512]{2,1,0:T(8,128)(2,1)S(1)} %copy-done), kind=kOutput, calls=%fused_computation.18 | convolution fusion | flops 2147483648 | bytes 8388608 | tf_op jit(solution)/shard_map/dot_general | solution.py:122
  112.1 3.7 %multiply_convert_fusion = bf16[1024,512]{1,0:T(8,128)(2,1)} fusion(f32[1024,512]{1,0:T(8,128)S(1)} %fusion.8, bf16[1024,2048]{1,0:T(8,128)(2,1)S(1)} %bitcast.87, bf16[1,2048,512]{2,1,0:T(8,128)(2,1)S(1)} %copy-done.24), kind=kOutput, calls=%fused_computation.22 | convolution fusion | flops 2150629376 | bytes 9437184 | tf_op jit(solution)/shard_map/dot_general | solution.py:121
  118.5 1.8 convert_multiply_fusion.4
  120.3 1.4 slice.277
  121.7 1.4 slice.278
  123.1 1.4 slice.276
  125.8 2.0 multiply_add_fusion.1
  127.8 1.6 slice.283
  129.4 1.6 slice.284
  132.4 1.8 multiply_add_fusion.2
  135.5 1.5 slice.288
  137.0 1.5 slice.292
  138.6 1.6 multiply_add_fusion.3
  140.2 1.5 slice.295
  141.6 1.4 slice.296
  143.1 1.4 slice.294
  144.5 1.4 slice.298
  146.0 1.4 multiply_add_fusion.4
  150.1 1.4 slice.300
  152.8 1.4 multiply_add_fusion.5
  158.1 1.4 multiply_add_fusion.6
  173.2 1.4 slice.293
  174.6 1.5 slice.326
  178.7 1.5 slice.287
  182.9 1.6 slice.330
  186.4 1.4 slice.275
  187.8 1.4 slice.332
  199.8 1.7 pad.114
  201.7 1.9 fusion.39
  204.4 12.8 %all-gather.1 = f32[8,1,512]{2,1,0:T(1,128)S(1)} all-gather(f32[1,1,512]{2,1,0:T(1,128)S(1)} %add_bitcast_fusion), channel_id=1, replica_groups=mesh['ep'=8,'tp'=4] {'ep'}, dimensions={0}, use_global_device_ids=true | all-gather | bytes 18432 | tf_op jit(solution)/shard_map/all_gather | solution.py:18
  217.2 1.7 pad.130
  218.9 1.6 pad.129
  221.3 12.8 %all-gather = f32[8,1,512]{2,1,0:T(1,128)S(1)} all-gather(f32[1,1,512]{2,1,0:T(1,128)S(1)} %add_bitcast_fusion.1), channel_id=1, replica_groups=mesh['ep'=8,'tp'=4] {'ep'}, dimensions={0}, use_global_device_ids=true | all-gather | bytes 18432 | tf_op jit(solution)/shard_map/all_gather | solution.py:18
  234.1 6.2 %fusion.14 = bf16[1024,512]{1,0:T(8,128)(2,1)} fusion(bf16[1024,2048]{1,0:T(8,128)(2,1)} %all-gather.7.cloned.1.call-done, bf16[1,2048,512]{2,1,0:T(8,128)(2,1)} %param.33), kind=kOutput, calls=%fused_computation.23 | convolution fusion | flops 2148007936 | bytes 7340032 | tf_op jit(solution)/shard_map/dot_general | solution.py:125
  240.3 3.9 %all-to-all-start.1 = ((bf16[8,128,512]{2,1,0:T(8,128)(2,1)}), bf16[8,128,512]{2,1,0:T(8,128)(2,1)S(1)}, u32[]{:S(2)}, u32[]{:S(2)}) async-start(bf16[8,128,512]{2,1,0:T(8,128)(2,1)} %bitcast.72), calls=%async_computation.1 | async-start | bytes 2097152 | tf_op jit(solution)/shard_map/all_to_all | solution.py:131
  244.7 4.1 %fusion.32 = bf16[256,512]{1,0:T(8,128)(2,1)} fusion(bf16[2048,512]{1,0:T(8,128)(2,1)} %param.21, f32[256,512]{1,0:T(8,128)} %pad.129, f32[256,512]{1,0:T(8,128)} %pad.130, f32[256,512]{1,0:T(8,128)} %copy-done.4, f32[256,512]{1,0:T(8,128)} %pad.114, bf16[256,2048]{1,0:T(8,128)(2,1)} %param.18, f32[2048]{0:T(1024)S(1)} %copy-done.28, ...), kind=kOutput, calls=%fused_computation.45 | convolution fusion | flops 541065216 | bytes 5516288 | tf_op jit(solution)/shard_map/dot_general | solution.py:68
  248.8 21.7 %all-to-all-done.1 = bf16[8,128,512]{2,1,0:T(8,128)(2,1)S(1)} async-done(((bf16[8,128,512]{2,1,0:T(8,128)(2,1)}), bf16[8,128,512]{2,1,0:T(8,128)(2,1)S(1)}, u32[]{:S(2)}, u32[]{:S(2)}) %all-to-all-start.1) | async-done | bytes 1048608 | tf_op jit(solution)/shard_map/all_to_all | solution.py:131
  270.5 2.6 gather_fusion.1
  273.1 1.7 reshape.120
  274.8 2.1 multiply_reduce_fusion
  (213 shorter events, 57.0 us)
Async XLA Ops:
  7.2 100.3 %copy-start = (bf16[1,2048,512]{2,1,0:T(8,128)(2,1)S(1)}, bf16[1,2048,512]{2,1,0:T(8,128)(2,1)}, u32[]{:S(2)}) copy-start(bf16[1,2048,512]{2,1,0:T(8,128)(2,1)} %param.32) | copy-start | bytes 6291460
  7.2 8.0 %copy-start.1 = (bf16[256,2048]{1,0:T(8,128)(2,1)S(1)}, bf16[256,2048]{1,0:T(8,128)(2,1)}, u32[]{:S(2)}) copy-start(bf16[256,2048]{1,0:T(8,128)(2,1)} %param.27) | copy-start | bytes 3145732
  7.2 8.0 %copy-start.12 = (f32[2048]{0:T(1024)S(1)}, f32[2048]{0:T(1024)}, u32[]{:S(2)}) copy-start(f32[2048]{0:T(1024)} %param.28) | copy-start | bytes 24580
  7.2 100.2 %all-gather.5.cloned.1.call-start = ((), (), s32[]{:S(2)}) async-start(), calls=%async_computation.2 | async-start | bytes 5242880 | tf_op jit(solution)/shard_map/all_gather | solution.py:117
  22.9 33.1 %copy-start.2 = (bf16[256,2048]{1,0:T(8,128)(2,1)S(1)}, bf16[256,2048]{1,0:T(8,128)(2,1)}, u32[]{:S(2)}) copy-start(bf16[256,2048]{1,0:T(8,128)(2,1)} %param.18) | copy-start | bytes 3145732
  22.9 33.9 %copy-start.27 = (f32[2048]{0:T(1024)S(1)}, f32[2048]{0:T(1024)}, u32[]{:S(2)}) copy-start(f32[2048]{0:T(1024)} %param.19) | copy-start | bytes 24580
  55.9 178.2 %all-gather.7.cloned.1.call-start = ((), (), s32[]{:S(2)}) async-start(), calls=%async_computation.3 | async-start | bytes 5242880 | tf_op jit(solution)/shard_map/all_gather | solution.py:126
  56.2 0.6 copy-start.21
  56.8 4.7 %copy-start.18 = (f32[256,2]{0,1:T(2,128)S(1)}, f32[256,2]{0,1:T(2,128)}, u32[]{:S(2)}) copy-start(f32[256,2]{0,1:T(2,128)} %param.30) | copy-start | bytes 6148
  56.8 4.7 %copy-start.20 = (f32[512]{0:T(512)S(1)}, f32[512]{0:T(512)}, u32[]{:S(2)}) copy-start(f32[512]{0:T(512)} %param.25) | copy-start | bytes 6148
  56.8 4.7 %copy-start.19 = (f32[4,512]{1,0:T(4,128)S(1)}, f32[4,512]{1,0:T(4,128)}, u32[]{:S(2)}) copy-start(f32[4,512]{1,0:T(4,128)} %param.22) | copy-start | bytes 24580
  59.2 0.7 copy-start.7
  59.9 3.0 %collective-permute-start = (bf16[3,512]{1,0:T(4,128)(2,1)S(1)}, bf16[3,512]{1,0:T(4,128)(2,1)S(1)}, u32[]{:S(2)}, u32[]{:S(2)}) collective-permute-start(bf16[3,512]{1,0:T(4,128)(2,1)S(1)} %slice.356), channel_id=1, source_target_pairs={{0,4},{4,8},{8,12},{12,16},{16,20},{20,24},{24,28},{1,5},{5,9},{9,... | collective-permute-start | bytes 9224 | tf_op jit(solution)/shard_map/ppermute | solution.py:13
  107.4 4.7 %copy-start.23 = (bf16[8,128,2048]{2,1,0:T(8,128)(2,1)S(1)}, bf16[8,128,2048]{2,1,0:T(8,128)(2,1)}, u32[]{:S(2)}) copy-start(bf16[8,128,2048]{2,1,0:T(8,128)(2,1)} %all-gather.5.cloned.1.call-done) | copy-start | bytes 12582916
  107.4 4.7 %copy-start.24 = (bf16[1,2048,512]{2,1,0:T(8,128)(2,1)S(1)}, bf16[1,2048,512]{2,1,0:T(8,128)(2,1)}, u32[]{:S(2)}) copy-start(bf16[1,2048,512]{2,1,0:T(8,128)(2,1)} %param.31) | copy-start | bytes 6291460
  112.1 3.7 %copy-start.25 = (bf16[4,128,128]{2,1,0:T(8,128)(2,1)S(1)}, bf16[4,128,128]{2,1,0:T(8,128)(2,1)}, u32[]{:S(2)}) copy-start(bf16[4,128,128]{2,1,0:T(8,128)(2,1)} %param.23) | copy-start | bytes 393220
  115.8 1.4 copy-start.26
  186.4 12.3 %copy-start.8 = (f32[31,512]{1,0:T(8,128)S(1)}, f32[31,512]{1,0:T(8,128)}, u32[]{:S(2)}) copy-start(f32[31,512]{1,0:T(8,128)} %slice.287) | copy-start | bytes 190468
  186.4 12.3 %copy-start.9 = (f32[31,512]{1,0:T(8,128)S(1)}, f32[31,512]{1,0:T(8,128)}, u32[]{:S(2)}) copy-start(f32[31,512]{1,0:T(8,128)} %slice.328) | copy-start | bytes 190468
  189.8 9.0 %copy-start.17 = (f32[1,512]{1,0:T(1,128)S(1)}, f32[1,512]{1,0:T(1,128)}, u32[]{:S(2)}) copy-start(f32[1,512]{1,0:T(1,128)} %slice.389) | copy-start | bytes 6148
  194.2 5.4 %copy-start.6 = (f32[63,512]{1,0:T(8,128)S(1)}, f32[63,512]{1,0:T(8,128)}, u32[]{:S(2)}) copy-start(f32[63,512]{1,0:T(8,128)} %slice.330) | copy-start | bytes 387076
  197.9 1.8 copy-start.16
  199.5 2.0 copy-start.15
  201.5 2.1 copy-start.14
  201.7 17.2 %copy-start.13 = (f32[1,512]{1,0:T(1,128)S(1)}, f32[1,512]{1,0:T(1,128)}, u32[]{:S(2)}) copy-start(f32[1,512]{1,0:T(1,128)} %slice.387) | copy-start | bytes 6148
  203.6 15.3 %copy-start.3 = (f32[127,512]{1,0:T(8,128)S(1)}, f32[127,512]{1,0:T(8,128)}, u32[]{:S(2)}) copy-start(f32[127,512]{1,0:T(8,128)} %get-tuple-element.130) | copy-start | bytes 780292
  203.7 36.6 %copy-start.4 = (f32[256,512]{1,0:T(8,128)}, f32[256,512]{1,0:T(8,128)S(1)}, u32[]{:S(2)}) copy-start(f32[256,512]{1,0:T(8,128)S(1)} %pad.113) | copy-start | bytes 1572868
  240.3 3.9 %copy-start.10 = (f32[512]{0:T(512)S(1)}, f32[512]{0:T(512)}, u32[]{:S(2)}) copy-start(f32[512]{0:T(512)} %custom-call) | copy-start | bytes 6148
  240.3 4.4 %copy-start.22 = (f32[256]{0:T(256)S(1)}, f32[256]{0:T(256)}, u32[]{:S(2)}) copy-start(f32[256]{0:T(256)} %copy-done.21) | copy-start | bytes 3076
  240.3 4.4 %copy-start.28 = (f32[2048]{0:T(1024)S(1)}, f32[2048]{0:T(1024)}, u32[]{:S(2)}) copy-start(f32[2048]{0:T(1024)} %param.19) | copy-start | bytes 24580
  240.3 30.2 %all-to-all-start.1 = ((bf16[8,128,512]{2,1,0:T(8,128)(2,1)}), bf16[8,128,512]{2,1,0:T(8,128)(2,1)S(1)}, u32[]{:S(2)}, u32[]{:S(2)}) async-start(bf16[8,128,512]{2,1,0:T(8,128)(2,1)} %bitcast.72), calls=%async_computation.1 | async-start | bytes 2097152 | tf_op jit(solution)/shard_map/all_to_all | solution.py:131
  244.7 25.8 %copy-start.11 = (s32[1024]{0:T(1024)S(1)}, s32[1024]{0:T(1024)}, u32[]{:S(2)}) copy-start(s32[1024]{0:T(1024)} %pad_clamp_fusion) | copy-start | bytes 12292
  270.5 4.3 %copy-start.5 = (f32[256,2]{1,0:T(8,128)S(1)}, f32[256,2]{1,0:T(8,128)}, u32[]{:S(2)}) copy-start(f32[256,2]{1,0:T(8,128)} %copy.41) | copy-start | bytes 6148
Sparse Core Ops, SparseCore 0:
  56.0 51.3 all-gather.4
  115.9 52.4 all-gather.6
where the time goes:
time: 286 us; the launch traced here: 284 us
  local copies, waits for them, and re-layouts  86.2 us (30%)
  waiting for transfers between devices  64.5 us (23%)
  blocking collectives  58.5 us (20%)
  other arithmetic  32.3 us (11%)
  matrix products  21.7 us (8%)
  between operations  14.8 us (5%)
  starting transfers between devices  5.54 us (2%)
    slice x52, local copies, waits for them, and re-layouts, local(): lax.associative_scan(link, (jnp.exp(log_decay), lru_drive), axis=0)  60.4 us
    all_gather x1, waiting for transfers between devices, local(): piece = lax.all_gather(incoming, 'tp', axis=2, tiled=True)  42.8 us
    all_to_all x1, blocking collectives, local(): lax.all_to_all(own_columns, 'ep', split_axis=0, concat_axis=0, tiled=True)  33 us
    all_gather x2, blocking collectives, entering(): everything = jax.tree.map(lambda part: lax.all_gather(part, axis), value)  25.6 us
    all_to_all x1, waiting for transfers between devices, local(): lax.all_to_all(results, 'ep', split_axis=0, concat_axis=0, tiled=True)  21.7 us
    add x13, other arithmetic, link(): return (earlier[0] * later[0], later[0] * earlier[1] + later[1])  14.6 us
    dot_general x1, matrix products, local(): jnp.dot(lax.all_gather(hidden, 'tp', axis=1, tiled=True), down_rows, pref...  6.22 us
    gather x1, local copies, waits for them, and re-layouts, local(): padded_rows[slot_owner].reshape(expert_count, capacity, feature_count)  5.98 us
  transfers between devices with their start and end apart: 4, of which 2 were waited for; matrix products, arithmetic and copies ran while one was open for 36% of the time, Pallas kernels for 0%

commit v1 on v0

--- a/solution.py
+++ b/solution.py
@@ -5,6 +5,20 @@
 
 epsilon = 1e-06
 lru_scale = 8.0
+
+
+def drive_streams_for(local_x, dim_i):
+    n_axis = lax.axis_size("tp")
+    answer = sorted(((i0, (i0 + 1) % n_axis) for i0 in range(n_axis)))
+    prior = local_x
+    buffer = [prior]
+    for hop_no in [*range(1, n_axis)]:
+        prior = lax.ppermute(prior, axis_name="tp", perm=answer)
+        buffer.insert(0, prior)
+    local_part = jnp.concatenate(buffer, axis=dim_i)
+    x_new = lax.axis_index("tp") + 1
+    outer = jnp.roll(local_part, shift=x_new * local_x.shape[dim_i], axis=dim_i)
+    return outer
 
 
 def from_behind(value, axis, by):
@@ -114,7 +128,7 @@
         outgoing, lax.axis_index("tp") * column_width, column_width, 2
     )
     incoming = lax.all_to_all(own_columns, "ep", split_axis=0, concat_axis=0, tiled=True)
-    piece = lax.all_gather(incoming, "tp", axis=2, tiled=True)
+    piece = drive_streams_for(incoming, 2)
     flat_rows = piece.reshape(slot_total, piece.shape[2])
     gate_rows = expert_gate[0]
     up_rows = expert_up[0]

time: 286 us -> 314 us (1.098)
  waiting for transfers between devices: 64.5 us -> 87.2 us
  local copies, waits for them, and re-layouts: 86.2 us -> 93.1 us
  matrix products: 21.7 us -> 17.7 us
    ppermute x0 -> x3, waiting for transfers between devices: none -> 65.5 us  [drive_streams_for(): prior = lax.ppermute(prior, axis_name='tp', perm=answer)]
    all_gather x1 -> x0, waiting for transfers between devices: 42.8 us -> none  [local(): piece = lax.all_gather(incoming, 'tp', axis=2, tiled=True)]
    unnamed x61 -> x72, local copies, waits for them, and re-layouts: 2.35 us -> 8.73 us
  transfers between devices with their start and end apart: 4 -> 6, of which waited for: 2 -> 4; matrix products, arithmetic and copies ran while one was open for 36% -> 32% of each run, Pallas kernels for 0% -> 0%
where the time goes in v1:
time: 314 us; the launch traced here: 311 us
  local copies, waits for them, and re-layouts  93.1 us (30%)
  waiting for transfers between devices  87.2 us (28%)
  blocking collectives  58.4 us (19%)
  other arithmetic  32.3 us (10%)
  matrix products  17.7 us (6%)
  between operations  14.9 us (5%)
  starting transfers between devices  7.5 us (2%)
    ppermute x3, waiting for transfers between devices, drive_streams_for(): prior = lax.ppermute(prior, axis_name='tp', perm=answer)  65.5 us
    slice x52, local copies, waits for them, and re-layouts, local(): lax.associative_scan(link, (jnp.exp(log_decay), lru_drive), axis=0)  60.4 us
    all_to_all x1, blocking collectives, local(): lax.all_to_all(own_columns, 'ep', split_axis=0, concat_axis=0, tiled=True)  32.8 us
    all_gather x2, blocking collectives, entering(): everything = jax.tree.map(lambda part: lax.all_gather(part, axis), value)  25.5 us
    all_to_all x1, waiting for transfers between devices, local(): lax.all_to_all(results, 'ep', split_axis=0, concat_axis=0, tiled=True)  21.7 us
    add x13, other arithmetic, link(): return (earlier[0] * later[0], later[0] * earlier[1] + later[1])  14.6 us
    unnamed x72, local copies, waits for them, and re-layouts  8.73 us
  transfers between devices with their start and end apart: 6, of which 4 were waited for; matrix products, arithmetic and copies ran while one was open for 32% of the time, Pallas kernels for 0%

profile of v1, /device:TPU:0, one launch (start us, length us, event | category | flops | bytes accessed | tf_op | source)
XLA Modules:
  0.0 311.3 jit_solution(8611729778208925656)
XLA Ops:
  11.2 2.4 scatter_custom_fusion
  13.6 1.5 fusion.3
  15.6 6.0 %gather_fusion = bf16[1024,2048]{1,0:T(8,128)(2,1)} fusion(bf16[257,2048]{1,0:T(8,128)(2,1)S(1)} %concatenate.69, s32[1024]{0:T(1024)S(1)} %fusion.50), kind=kCustom, calls=%fused_computation | custom fusion | bytes 8392704 | tf_op jit(solution)/shard_map/gather | solution.py:125
  21.5 1.4 constant_dynamic-slice_fusion.3
  23.0 32.8 %all_to_all.10 = bf16[8,128,512]{2,1,0:T(8,128)(2,1)S(1)} all-to-all(bf16[8,128,512]{2,1,0:T(8,128)(2,1)S(1)} %constant_dynamic-slice_fusion.3), channel_id=1, replica_groups=mesh['ep'=8,'tp'=4] {'ep'}, dimensions={0} | all-to-all | bytes 2097152 | tf_op jit(solution)/shard_map/all_to_all | solution.py:130
  55.8 1.5 collective-permute-start.1
  57.3 23.9 %collective-permute-done.1 = bf16[8,128,512]{2,1,0:T(8,128)(2,1)S(1)} collective-permute-done((bf16[8,128,512]{2,1,0:T(8,128)(2,1)S(1)}, bf16[8,128,512]{2,1,0:T(8,128)(2,1)S(1)}, u32[]{:S(2)}, u32[]{:S(2)}) %collective-permute-start.1) | collective-permute-done | bytes 1048608 | tf_op jit(solution)/shard_map/ppermute | solution.py:16
  83.2 23.7 %collective-permute-done.2 = bf16[8,128,512]{2,1,0:T(8,128)(2,1)} collective-permute-done((bf16[8,128,512]{2,1,0:T(8,128)(2,1)S(1)}, bf16[8,128,512]{2,1,0:T(8,128)(2,1)}, u32[]{:S(2)}, u32[]{:S(2)}) %collective-permute-start.2) | collective-permute-done | bytes 1048608 | tf_op jit(solution)/shard_map/ppermute | solution.py:16
  108.4 1.5 collective-permute-start
  111.4 1.7 add_convert_fusion
  113.1 17.9 %collective-permute-done.3 = bf16[8,128,512]{2,1,0:T(8,128)(2,1)} collective-permute-done((bf16[8,128,512]{2,1,0:T(8,128)(2,1)}, bf16[8,128,512]{2,1,0:T(8,128)(2,1)}, u32[]{:S(2)}, u32[]{:S(2)}) %collective-permute-start.3) | collective-permute-done | bytes 1048608 | tf_op jit(solution)/shard_map/ppermute | solution.py:16
  134.0 1.4 constant_dynamic-update-slice_fusion.3
  137.5 2.3 fusion.10
  139.8 3.6 %multiply_convert_fusion = bf16[1024,512]{1,0:T(8,128)(2,1)} fusion(f32[1024,512]{1,0:T(8,128)S(1)} %fusion.10, bf16[1024,2048]{1,0:T(8,128)(2,1)S(1)} %bitcast.73, bf16[1,2048,512]{2,1,0:T(8,128)(2,1)S(1)} %copy-done.26), kind=kOutput, calls=%fused_computation.22 | convolution fusion | flops 2150629376 | bytes 9437184 | tf_op jit(solution)/shard_map/dot_general | solution.py:136
  146.2 1.8 convert_multiply_fusion.4
  147.9 1.4 slice.277
  153.4 2.0 multiply_add_fusion.1
  155.5 1.6 slice.283
  157.1 1.6 slice.284
  160.1 1.8 multiply_add_fusion.2
  163.1 1.5 slice.288
  164.6 1.5 slice.292
  166.2 1.6 multiply_add_fusion.3
  167.8 1.4 slice.295
  169.2 1.4 slice.296
  170.7 1.4 slice.294
  172.1 1.4 slice.298
  173.6 1.4 multiply_add_fusion.4
  185.7 1.4 multiply_add_fusion.6
  200.8 1.4 slice.293
  202.3 1.4 slice.326
  206.3 1.5 slice.287
  210.5 1.6 slice.330
  214.0 1.4 slice.275
  215.4 1.4 slice.332
  227.4 1.6 pad.114
  229.3 1.9 fusion.39
  232.0 12.8 %all-gather.1 = f32[8,1,512]{2,1,0:T(1,128)S(1)} all-gather(f32[1,1,512]{2,1,0:T(1,128)S(1)} %add_bitcast_fusion), channel_id=1, replica_groups=mesh['ep'=8,'tp'=4] {'ep'}, dimensions={0}, use_global_device_ids=true | all-gather | bytes 18432 | tf_op jit(solution)/shard_map/all_gather | solution.py:32
  244.8 1.7 pad.130
  246.5 1.6 pad.129
  248.9 12.8 %all-gather = f32[8,1,512]{2,1,0:T(1,128)S(1)} all-gather(f32[1,1,512]{2,1,0:T(1,128)S(1)} %add_bitcast_fusion.1), channel_id=1, replica_groups=mesh['ep'=8,'tp'=4] {'ep'}, dimensions={0}, use_global_device_ids=true | all-gather | bytes 18432 | tf_op jit(solution)/shard_map/all_gather | solution.py:32
  261.6 6.2 %fusion.14 = bf16[1024,512]{1,0:T(8,128)(2,1)} fusion(bf16[1024,2048]{1,0:T(8,128)(2,1)} %all-gather.4.cloned.1.call-done, bf16[1,2048,512]{2,1,0:T(8,128)(2,1)} %param.33), kind=kOutput, calls=%fused_computation.23 | convolution fusion | flops 2148007936 | bytes 7340032 | tf_op jit(solution)/shard_map/dot_general | solution.py:139
  267.9 3.9 %all-to-all-start.1 = ((bf16[8,128,512]{2,1,0:T(8,128)(2,1)}), bf16[8,128,512]{2,1,0:T(8,128)(2,1)S(1)}, u32[]{:S(2)}, u32[]{:S(2)}) async-start(bf16[8,128,512]{2,1,0:T(8,128)(2,1)} %bitcast.74), calls=%async_computation.1 | async-start | bytes 2097152 | tf_op jit(solution)/shard_map/all_to_all | solution.py:145
  272.3 4.1 %fusion.32 = bf16[256,512]{1,0:T(8,128)(2,1)} fusion(bf16[2048,512]{1,0:T(8,128)(2,1)} %param.21, f32[256,512]{1,0:T(8,128)} %pad.129, f32[256,512]{1,0:T(8,128)} %pad.130, f32[256,512]{1,0:T(8,128)} %copy-done.6, f32[256,512]{1,0:T(8,128)} %pad.114, bf16[256,2048]{1,0:T(8,128)(2,1)} %param.18, f32[2048]{0:T(1024)S(1)} %copy-done.30, ...), kind=kOutput, calls=%fused_computation.45 | convolution fusion | flops 541065216 | bytes 5516288 | tf_op jit(solution)/shard_map/dot_general | solution.py:82
  276.4 21.7 %all-to-all-done.1 = bf16[8,128,512]{2,1,0:T(8,128)(2,1)S(1)} async-done(((bf16[8,128,512]{2,1,0:T(8,128)(2,1)}), bf16[8,128,512]{2,1,0:T(8,128)(2,1)S(1)}, u32[]{:S(2)}, u32[]{:S(2)}) %all-to-all-start.1) | async-done | bytes 1048608 | tf_op jit(solution)/shard_map/all_to_all | solution.py:145
  298.1 2.6 gather_fusion.1
  300.7 1.7 reshape.120
  302.4 2.1 multiply_reduce_fusion
  (229 shorter events, 67.9 us)
Async XLA Ops:
  7.2 130.3 %copy-start = (bf16[1,2048,512]{2,1,0:T(8,128)(2,1)S(1)}, bf16[1,2048,512]{2,1,0:T(8,128)(2,1)}, u32[]{:S(2)}) copy-start(bf16[1,2048,512]{2,1,0:T(8,128)(2,1)} %param.31) | copy-start | bytes 6291460
  7.2 8.0 %copy-start.1 = (bf16[256,2048]{1,0:T(8,128)(2,1)S(1)}, bf16[256,2048]{1,0:T(8,128)(2,1)}, u32[]{:S(2)}) copy-start(bf16[256,2048]{1,0:T(8,128)(2,1)} %param.27) | copy-start | bytes 3145732
  7.2 8.0 %copy-start.14 = (f32[2048]{0:T(1024)S(1)}, f32[2048]{0:T(1024)}, u32[]{:S(2)}) copy-start(f32[2048]{0:T(1024)} %param.28) | copy-start | bytes 24580
  7.2 254.4 %all-gather.4.cloned.1.call-start = ((), (), s32[]{:S(2)}) async-start(), calls=%async_computation.2 | async-start | bytes 5242880 | tf_op jit(solution)/shard_map/all_gather | solution.py:140
  21.5 61.3 %copy-start.4 = (bf16[256,2048]{1,0:T(8,128)(2,1)S(1)}, bf16[256,2048]{1,0:T(8,128)(2,1)}, u32[]{:S(2)}) copy-start(bf16[256,2048]{1,0:T(8,128)(2,1)} %param.18) | copy-start | bytes 3145732
  23.0 84.0 %copy-start.25 = (bf16[2048,512]{1,0:T(8,128)(2,1)S(1)}, bf16[2048,512]{1,0:T(8,128)(2,1)}, u32[]{:S(2)}) copy-start(bf16[2048,512]{1,0:T(8,128)(2,1)} %param.20) | copy-start | bytes 6291460
  23.0 84.0 %copy-start.29 = (f32[2048]{0:T(1024)S(1)}, f32[2048]{0:T(1024)}, u32[]{:S(2)}) copy-start(f32[2048]{0:T(1024)} %param.19) | copy-start | bytes 24580
  55.8 25.4 %collective-permute-start.1 = (bf16[8,128,512]{2,1,0:T(8,128)(2,1)S(1)}, bf16[8,128,512]{2,1,0:T(8,128)(2,1)S(1)}, u32[]{:S(2)}, u32[]{:S(2)}) collective-permute-start(bf16[8,128,512]{2,1,0:T(8,128)(2,1)S(1)} %all_to_all.10), channel_id=1, source_target_pairs={{0,1},{1,2},{2,3},{3,0},{4,5},{5,6},{6,7},{7,4},{8,9},{9,10},{10,1... | collective-permute-start | bytes 3145736 | tf_op jit(solution)/shard_map/ppermute | solution.py:16
  81.3 1.0 copy-start.2
  82.2 24.7 %collective-permute-start.2 = (bf16[8,128,512]{2,1,0:T(8,128)(2,1)S(1)}, bf16[8,128,512]{2,1,0:T(8,128)(2,1)}, u32[]{:S(2)}, u32[]{:S(2)}) collective-permute-start(bf16[8,128,512]{2,1,0:T(8,128)(2,1)S(1)} %collective-permute-done.1), channel_id=1, source_target_pairs={{0,1},{1,2},{2,3},{3,0},{4,5},{5,6},{6,7},{7,4},{8,9},{9,10},{10,1... | collective-permute-start | bytes 3145736 | tf_op jit(solution)/shard_map/ppermute | solution.py:16
  83.1 23.8 %copy-start.23 = (f32[256]{0:T(256)}, f32[256]{0:T(256)S(1)}, u32[]{:S(2)}) copy-start(f32[256]{0:T(256)S(1)} %add_rsqrt_fusion.1) | copy-start | bytes 3076
  83.1 26.7 %copy-start.20 = (f32[256,2]{0,1:T(2,128)S(1)}, f32[256,2]{0,1:T(2,128)}, u32[]{:S(2)}) copy-start(f32[256,2]{0,1:T(2,128)} %param.30) | copy-start | bytes 6148
  83.1 26.8 %copy-start.22 = (f32[512]{0:T(512)S(1)}, f32[512]{0:T(512)}, u32[]{:S(2)}) copy-start(f32[512]{0:T(512)} %param.25) | copy-start | bytes 6148
  83.2 26.8 %copy-start.21 = (f32[4,512]{1,0:T(4,128)S(1)}, f32[4,512]{1,0:T(4,128)}, u32[]{:S(2)}) copy-start(f32[4,512]{1,0:T(4,128)} %param.22) | copy-start | bytes 24580
  106.9 24.0 %collective-permute-start.3 = (bf16[8,128,512]{2,1,0:T(8,128)(2,1)}, bf16[8,128,512]{2,1,0:T(8,128)(2,1)}, u32[]{:S(2)}, u32[]{:S(2)}) collective-permute-start(bf16[8,128,512]{2,1,0:T(8,128)(2,1)} %collective-permute-done.2), channel_id=1, source_target_pairs={{0,1},{1,2},{2,3},{3,0},{4,5},{5,6},{6,7},{7,4},{8,9},{9,10},{10,1... | collective-permute-start | bytes 3145736 | tf_op jit(solution)/shard_map/ppermute | solution.py:16
  107.7 0.7 copy-start.9
  108.4 3.0 collective-permute-start
  113.1 20.6 %copy-start.3 = (bf16[8,128,512]{2,1,0:T(8,128)(2,1)S(1)}, bf16[8,128,512]{2,1,0:T(8,128)(2,1)}, u32[]{:S(2)}) copy-start(bf16[8,128,512]{2,1,0:T(8,128)(2,1)} %copy-done.2) | copy-start | bytes 3145732
  137.5 2.3 copy-start.26
  139.8 3.6 %copy-start.27 = (bf16[4,128,128]{2,1,0:T(8,128)(2,1)S(1)}, bf16[4,128,128]{2,1,0:T(8,128)(2,1)}, u32[]{:S(2)}) copy-start(bf16[4,128,128]{2,1,0:T(8,128)(2,1)} %param.23) | copy-start | bytes 393220
  143.4 1.4 copy-start.28
  214.0 12.3 %copy-start.10 = (f32[31,512]{1,0:T(8,128)S(1)}, f32[31,512]{1,0:T(8,128)}, u32[]{:S(2)}) copy-start(f32[31,512]{1,0:T(8,128)} %slice.287) | copy-start | bytes 190468
  214.0 12.3 %copy-start.11 = (f32[31,512]{1,0:T(8,128)S(1)}, f32[31,512]{1,0:T(8,128)}, u32[]{:S(2)}) copy-start(f32[31,512]{1,0:T(8,128)} %slice.328) | copy-start | bytes 190468
  217.4 8.9 %copy-start.19 = (f32[1,512]{1,0:T(1,128)S(1)}, f32[1,512]{1,0:T(1,128)}, u32[]{:S(2)}) copy-start(f32[1,512]{1,0:T(1,128)} %slice.389) | copy-start | bytes 6148
  221.8 5.4 %copy-start.8 = (f32[63,512]{1,0:T(8,128)S(1)}, f32[63,512]{1,0:T(8,128)}, u32[]{:S(2)}) copy-start(f32[63,512]{1,0:T(8,128)} %slice.330) | copy-start | bytes 387076
  225.5 1.8 copy-start.18
  227.2 1.9 copy-start.17
  229.1 2.1 copy-start.16
  229.2 17.2 %copy-start.15 = (f32[1,512]{1,0:T(1,128)S(1)}, f32[1,512]{1,0:T(1,128)}, u32[]{:S(2)}) copy-start(f32[1,512]{1,0:T(1,128)} %slice.387) | copy-start | bytes 6148
  231.1 15.3 %copy-start.5 = (f32[127,512]{1,0:T(8,128)S(1)}, f32[127,512]{1,0:T(8,128)}, u32[]{:S(2)}) copy-start(f32[127,512]{1,0:T(8,128)} %get-tuple-element.130) | copy-start | bytes 780292
  231.3 36.6 %copy-start.6 = (f32[256,512]{1,0:T(8,128)}, f32[256,512]{1,0:T(8,128)S(1)}, u32[]{:S(2)}) copy-start(f32[256,512]{1,0:T(8,128)S(1)} %pad.113) | copy-start | bytes 1572868
  267.9 3.9 %copy-start.12 = (f32[512]{0:T(512)S(1)}, f32[512]{0:T(512)}, u32[]{:S(2)}) copy-start(f32[512]{0:T(512)} %custom-call) | copy-start | bytes 6148
  267.9 4.4 %copy-start.24 = (f32[256]{0:T(256)S(1)}, f32[256]{0:T(256)}, u32[]{:S(2)}) copy-start(f32[256]{0:T(256)} %copy-done.23) | copy-start | bytes 3076
  267.9 4.4 %copy-start.30 = (f32[2048]{0:T(1024)S(1)}, f32[2048]{0:T(1024)}, u32[]{:S(2)}) copy-start(f32[2048]{0:T(1024)} %param.19) | copy-start | bytes 24580
  267.9 30.2 %all-to-all-start.1 = ((bf16[8,128,512]{2,1,0:T(8,128)(2,1)}), bf16[8,128,512]{2,1,0:T(8,128)(2,1)S(1)}, u32[]{:S(2)}, u32[]{:S(2)}) async-start(bf16[8,128,512]{2,1,0:T(8,128)(2,1)} %bitcast.74), calls=%async_computation.1 | async-start | bytes 2097152 | tf_op jit(solution)/shard_map/all_to_all | solution.py:145
  272.3 25.8 %copy-start.13 = (s32[1024]{0:T(1024)S(1)}, s32[1024]{0:T(1024)}, u32[]{:S(2)}) copy-start(s32[1024]{0:T(1024)} %pad_clamp_fusion) | copy-start | bytes 12292
  298.1 4.3 %copy-start.7 = (f32[256,2]{1,0:T(8,128)S(1)}, f32[256,2]{1,0:T(8,128)}, u32[]{:S(2)}) copy-start(f32[256,2]{1,0:T(8,128)} %copy.41) | copy-start | bytes 6148
Sparse Core Ops, SparseCore 0:
  143.6 52.2 all-gather.3
